TPU v7x, 32 devices: a whole 2x2x4 slice. The times are simulated.
32 devices in a mesh: sp: 4 (over y, x), tp: 8 (over z, core).
Axes of the slice: x: 2, y: 2, z: 4, core: 2. Of those that a mesh axis runs over, the one named last changes fastest.
Arguments:
- query_a: bfloat16 [512, 16, 256], P('sp', 'tp'), may hold values from -5.5 to 5.5
- key_a: bfloat16 [512, 16, 256], P('sp', 'tp'), may hold values from -5.5 to 5.5
- value_a: bfloat16 [512, 16, 256], P('sp', 'tp'), may hold values from -6 to 6
- query_b: bfloat16 [512, 16, 128], P('sp', 'tp'), may hold values from -5.5 to 5.5
- key_b: bfloat16 [512, 16, 128], P('sp', 'tp'), may hold values from -5.5 to 5.5
- value_b: bfloat16 [512, 16, 128], P('sp', 'tp'), may hold values from -6 to 6
- lambdas: float32 [2, 16], P(None, 'tp'), may hold values from 0.3 to 0.8
- gain_a: float32 [256], replicated, may hold values from 0.1 to 1.9
- gain_b: float32 [128], replicated, may hold values from 0.1 to 1.9
- out_a: bfloat16 [4096, 4096], P('tp'), may hold values from -0.078125 to 0.078125
- out_b: bfloat16 [2048, 4096], P('tp'), may hold values from -0.078125 to 0.078125
- residual: bfloat16 [512, 4096], P(('sp', 'tp')), may hold values from -6 to 6
- norm_gain: float32 [4096], replicated, may hold values from 0.1 to 1.9
- route_ids: int32 [512, 2], P(('sp', 'tp')), may hold values from 0 to 7, all different within a row; in each aligned block of 16 rows (0 to 15, 16 to 31, ...) at most 8 rows name the same one
- route_weights: float32 [512, 2], P(('sp', 'tp')), may hold values from 0.1 to 0.9
- w_gate: bfloat16 [8, 4096, 2048], P('sp', None, 'tp'), may hold values from -0.28125 to 0.28125
- w_up: bfloat16 [8, 4096, 2048], P('sp', None, 'tp'), may hold values from -0.28125 to 0.28125
- w_down: bfloat16 [8, 2048, 4096], P('sp', 'tp'), may hold values from -0.01977539 to 0.01977539
Outputs:
- result: bfloat16 [512, 4096], P(('sp', 'tp'))
Inputs may be any that keep to these rules, and one draw needn't show every extreme that they name: `route_ids`: in the rows of one device each token names 2 different experts, no expert is named more than 8 times, a bound that some block reaches.
All inputs are finite; a program needn't handle non-finite values.
Results may differ from a plain program's by a relative error of at most 0.02.
Values may be sent and summed in bfloat16 or wider, within the bound.
A program may use at most 128 MiB of HBM per device.

v0:
```python
import jax
import jax.numpy as jnp
from jax import lax
from jax.sharding import PartitionSpec as P

EPSILON = 1e-06
LIMIT = 7.0
SLOPE = 1.702
FLOOR = -1e30


def empty_state(heads_here, queries_here, value_width):
    maxima = jnp.full((2, heads_here, queries_here), FLOOR, jnp.float32)
    totals = jnp.zeros((2, heads_here, queries_here), jnp.float32)
    sums = jnp.zeros((2, heads_here, queries_here, value_width), jnp.float32)
    return (maxima, totals, sums)


def absorb_keys(states, queries, keys, values, width):
    maxima, totals, sums = states
    scaling = width ** (-0.5)
    new_maxima = []
    new_totals = []
    new_sums = []
    for which in range(2):
        query_part = queries[:, :, which * width : (which + 1) * width]
        key_part = keys[:, :, which * width : (which + 1) * width]
        scores = (
            jnp.einsum("qhd,khd->hqk", query_part, key_part, preferred_element_type=jnp.float32)
            * scaling
        )
        highest = jnp.maximum(maxima[which], jnp.max(scores, axis=2))
        expo = jnp.exp(scores - highest[:, :, None])
        factor = jnp.exp(maxima[which] - highest)
        new_totals.append(totals[which] * factor + jnp.sum(expo, axis=2))
        carried = jnp.einsum(
            "hqk,khv->hqv", expo.astype(jnp.bfloat16), values, preferred_element_type=jnp.float32
        )
        new_sums.append(sums[which] * factor[:, :, None] + carried)
        new_maxima.append(highest)
    return (jnp.stack(new_maxima), jnp.stack(new_totals), jnp.stack(new_sums))


def finish(states, lambda_row, gain):
    maxima, totals, sums = states
    heard = sums / totals[:, :, :, None]
    differ = heard[0] - lambda_row[:, None, None] * heard[1]
    scaled = lax.rsqrt(jnp.mean(differ * differ, axis=2, keepdims=True) + EPSILON)
    return (differ * scaled * gain).astype(jnp.bfloat16)


def gated_units(grid, w_gate, w_up):
    gate = jnp.einsum("necd,edf->necf", grid, w_gate, preferred_element_type=jnp.float32)
    upward = jnp.einsum("necd,edf->necf", grid, w_up, preferred_element_type=jnp.float32)
    clamped = jnp.minimum(gate, LIMIT)
    return (
        clamped * jax.nn.sigmoid(SLOPE * clamped) * (jnp.clip(upward, -LIMIT, LIMIT) + 1.0)
    ).astype(jnp.bfloat16)


def per_device(
    query_a,
    key_a,
    value_a,
    query_b,
    key_b,
    value_b,
    lambdas,
    gain_a,
    gain_b,
    out_a,
    out_b,
    residual,
    norm_gain,
    route_ids,
    route_weights,
    w_gate,
    w_up,
    w_down,
):
    heads_here = query_a.shape[1]
    queries_here = query_a.shape[0]
    width_a = query_a.shape[2] // 2
    width_b = query_b.shape[2] // 2
    starting = (
        empty_state(heads_here, queries_here, value_a.shape[2]),
        empty_state(heads_here, queries_here, value_b.shape[2]),
    )
    keys_a = lax.all_gather(key_a, "sp", axis=0, tiled=True)
    values_a = lax.all_gather(value_a, "sp", axis=0, tiled=True)
    keys_b = lax.all_gather(key_b, "sp", axis=0, tiled=True)
    values_b = lax.all_gather(value_b, "sp", axis=0, tiled=True)
    state_a = absorb_keys(starting[0], query_a, keys_a, values_a, width_a)
    state_b = absorb_keys(starting[1], query_b, keys_b, values_b, width_b)
    attended_a = finish(state_a, lambdas[0], gain_a)
    attended_b = finish(state_b, lambdas[1], gain_b)
    model_width = out_a.shape[1]
    weights_a = out_a.reshape(heads_here, -1, model_width)
    weights_b = out_b.reshape(heads_here, -1, model_width)
    first = jnp.einsum("hqv,hvd->qd", attended_a, weights_a, preferred_element_type=jnp.float32)
    projected = lax.psum_scatter(
        (
            first
            + jnp.einsum("hqv,hvd->qd", attended_b, weights_b, preferred_element_type=jnp.float32)
        ).astype(jnp.bfloat16),
        "tp",
        scatter_dimension=0,
        tiled=True,
    ).astype(jnp.float32)
    mixed = (residual.astype(jnp.float32) + projected).astype(jnp.bfloat16)
    widened = mixed.astype(jnp.float32)
    normed = (
        widened
        * lax.rsqrt(jnp.mean(widened * widened, axis=1, keepdims=True) + EPSILON)
        * norm_gain
    ).astype(jnp.bfloat16)
    rows_here, chosen = route_ids.shape
    groups = lax.axis_size("sp")
    experts_here = w_gate.shape[0]
    experts_all = experts_here * groups
    capacity = 2 * rows_here * chosen // experts_all
    slots_here = experts_here * capacity
    flat_ids = route_ids.reshape(-1)
    onehot = (flat_ids[:, None] == jnp.arange(experts_all, dtype=jnp.int32)[None, :]).astype(
        jnp.int32
    )
    earlier = jnp.cumsum(onehot, axis=0) - onehot
    target = flat_ids * capacity + jnp.sum(earlier * onehot, axis=1)
    places = jnp.arange(experts_all * capacity, dtype=jnp.int32)
    layout = jnp.any(target.reshape(rows_here, chosen)[None, :, :] == places[:, None, None], axis=2)
    outgoing = jnp.dot(
        layout.astype(jnp.bfloat16), normed, preferred_element_type=jnp.float32
    ).astype(jnp.bfloat16)
    outgoing = outgoing.reshape(groups, slots_here, model_width)
    arrived = lax.all_to_all(outgoing, "sp", split_axis=0, concat_axis=0, tiled=True)
    pieces = lax.all_gather(arrived, "tp", axis=0, tiled=True)
    count = pieces.shape[0]
    grid = pieces.reshape(count, experts_here, capacity, model_width)
    active = gated_units(grid, w_gate, w_up)
    down = jnp.einsum("necf,efd->necd", active, w_down, preferred_element_type=jnp.float32)
    partial_value = down.astype(jnp.bfloat16).reshape(count, slots_here, model_width)
    totals = lax.psum_scatter(
        partial_value.astype(jnp.float32).astype(jnp.bfloat16),
        "tp",
        scatter_dimension=0,
        tiled=True,
    )
    summed = lax.all_to_all(totals, "sp", split_axis=0, concat_axis=0, tiled=True)
    results = summed.reshape(experts_all * capacity, model_width)
    picked = (
        jnp.take(results, target, axis=0)
        .reshape(rows_here, chosen, model_width)
        .astype(jnp.float32)
    )
    combined = jnp.sum(route_weights[:, :, None] * picked, axis=1)
    return (widened + combined).astype(jnp.bfloat16)


def solution(mesh):
    in_specs = (
        P("sp", "tp", None),
        P("sp", "tp", None),
        P("sp", "tp", None),
        P("sp", "tp", None),
        P("sp", "tp", None),
        P("sp", "tp", None),
        P(None, "tp"),
        P(),
        P(),
        P("tp", None),
        P("tp", None),
        P(("sp", "tp"), None),
        P(),
        P(("sp", "tp"), None),
        P(("sp", "tp"), None),
        P("sp", None, "tp"),
        P("sp", None, "tp"),
        P("sp", "tp", None),
    )
    out_specs = P(("sp", "tp"), None)
    return jax.shard_map(
        per_device, mesh=mesh, in_specs=in_specs, out_specs=out_specs, check_vma=False
    )
```

profile of v0, /device:TPU:0, one launch (start us, length us, event | category | flops | bytes accessed | tf_op | source)
XLA Modules:
  0.0 234.9 jit_solution(8185951982461286773)
XLA Ops:
  6.5 1.1 copy.77
  7.6 11.5 %all_gather.15 = bf16[512,2,256]{2,0,1:T(8,128)(2,1)S(1)} all-gather(bf16[128,2,256]{2,0,1:T(8,128)(2,1)S(1)} %copy.77), channel_id=1, replica_groups=mesh['sp'=4,'tp'=8] {'sp'}, dimensions={0}, use_global_device_ids=true | all-gather | bytes 655360 | tf_op jit(solution)/shard_map/all_gather | solution.py:89
  19.1 1.0 fusion.120
  20.1 0.0 copy-start.6
  20.2 0.3 fusion.125
  20.5 0.3 fusion.124
  20.8 1.0 copy.78
  21.8 10.2 %all_gather.16 = bf16[512,2,256]{2,0,1:T(8,128)(2,1)S(1)} all-gather(bf16[128,2,256]{2,0,1:T(8,128)(2,1)S(1)} %copy.78), channel_id=1, replica_groups=mesh['sp'=4,'tp'=8] {'sp'}, dimensions={0}, use_global_device_ids=true | all-gather | bytes 655360 | tf_op jit(solution)/shard_map/all_gather | solution.py:90
  31.9 0.2 fusion.59
  32.2 0.2 fusion.61
  32.4 0.3 fusion.50
  32.7 0.3 fusion.49
  33.0 0.0 copy-start.14
  33.1 0.1 maximum_divide_fusion
  33.2 0.8 copy-done.2
  34.0 0.2 fusion.79
  34.2 0.1 copy.81
  34.3 8.6 %all_gather.17 = bf16[512,2,128]{0,2,1:T(8,128)(2,1)S(1)} all-gather(bf16[128,2,128]{0,2,1:T(8,128)(2,1)S(1)} %copy.81), channel_id=1, replica_groups=mesh['sp'=4,'tp'=8] {'sp'}, dimensions={0}, use_global_device_ids=true | all-gather | bytes 327680 | tf_op jit(solution)/shard_map/all_gather | solution.py:91
  42.9 0.1 fusion.121
  43.0 0.3 fusion.123
  43.3 0.3 fusion.122
  43.6 0.1 copy.82
  43.8 0.0 copy-start.11
  43.8 9.0 %all_gather.18 = bf16[512,2,128]{0,2,1:T(8,128)(2,1)S(1)} all-gather(bf16[128,2,128]{0,2,1:T(8,128)(2,1)S(1)} %copy.82), channel_id=1, replica_groups=mesh['sp'=4,'tp'=8] {'sp'}, dimensions={0}, use_global_device_ids=true | all-gather | bytes 327680 | tf_op jit(solution)/shard_map/all_gather | solution.py:92
  52.8 0.2 fusion.63
  53.1 0.2 fusion.65
  53.3 0.3 fusion.52
  53.6 0.3 fusion.51
  54.0 0.1 fusion.96
  54.1 0.6 convolution_bitcast_fusion
  54.7 0.0 copy-start.9
  54.7 1.8 fusion.2
  56.6 0.0 reduce-scatter.3.cloned.1.call-update
  56.6 0.0 all-gather.2.cloned.1.call-start
  56.7 0.1 copy.86
  56.7 0.1 reshape.254
  56.8 0.1 fusion.111
  56.9 0.1 reduce_window_sum.11
  57.0 0.2 select_reduce_fusion
  57.1 0.1 reduce_sum.104
  57.2 0.1 copy.87
  57.3 0.1 fusion.112
  57.4 32.2 %reduce-scatter.3.cloned.1.call-done = bf16[16,4096]{1,0:T(8,128)(2,1)} async-done(((bf16[128,4096]{1,0:T(8,128)(2,1)}), bf16[16,4096]{1,0:T(8,128)(2,1)}) %reduce-scatter.3.cloned.1.call-update) | async-done | bytes 131088 | tf_op jit(solution)/shard_map/reduce_scatter | solution.py:101
  89.6 1.1 fusion.67
  90.7 1.2 convolution_convert_fusion.1
  91.9 11.0 %all_to_all.10 = bf16[4,16,4096]{2,1,0:T(8,128)(2,1)} all-to-all(bf16[4,16,4096]{2,1,0:T(8,128)(2,1)S(1)} %bitcast.129), channel_id=1, replica_groups=mesh['sp'=4,'tp'=8] {'sp'}, dimensions={0} | all-to-all | bytes 1048576 | tf_op jit(solution)/shard_map/all_to_all | solution.py:135
  102.9 0.0 all-gather.2.cloned.1.call-update
  102.9 0.0 reduce-scatter.5.cloned.1.call-start
  103.0 45.4 %all-gather.2.cloned.1.call-done = bf16[32,16,4096]{2,1,0:T(8,128)(2,1)} async-done(((bf16[4,16,4096]{2,1,0:T(8,128)(2,1)}), bf16[32,16,4096]{2,1,0:T(8,128)(2,1)}) %all-gather.2.cloned.1.call-update) | async-done | bytes 4194320 | tf_op jit(solution)/shard_map/all_gather | solution.py:136
  148.3 4.7 %fusion.15 = f32[32,2,8,256]{3,2,0,1:T(8,128)S(1)} fusion(bf16[2,4096,256]{2,1,0:T(8,128)(2,1)} %param.33, bf16[32,16,4096]{2,1,0:T(8,128)(2,1)} %all-gather.2.cloned.1.call-done), kind=kOutput, calls=%fused_computation.21 | convolution fusion | flops 1073872896 | bytes 8912896 | tf_op jit(solution)/shard_map/necd,edf->necf/dot_general | solution.py:53
  153.1 9.1 %fusion = bf16[32,2,8,4096]{3,2,0,1:T(8,128)(2,1)} fusion(bf16[2,256,4096]{2,1,0:T(8,128)(2,1)} %param.35, bf16[2,4096,256]{2,1,0:T(8,128)(2,1)} %param.34, f32[32,2,8,256]{3,2,0,1:T(8,128)S(1)} %fusion.15, bf16[32,16,4096]{2,1,0:T(8,128)(2,1)} %all-gather.2.cloned.1.call-done), kind=kOutput, calls=%fused_computation.2 | convolution fusion | flops 2150760448 | bytes 17301504 | tf_op jit(solution)/shard_map/necf,efd->necd/dot_general | solution.py:140
  162.2 4.6 %copy.138 = bf16[32,2,8,4096]{3,2,1,0:T(8,128)(2,1)} copy(bf16[32,2,8,4096]{3,2,0,1:T(8,128)(2,1)} %fusion) | data formatting | bytes 8388608 | tf_op jit(solution)/shard_map/convert_element_type | solution.py:141
  166.8 0.0 reduce-scatter.5.cloned.1.call-update
  166.8 48.9 %reduce-scatter.5.cloned.1.call-done = bf16[4,16,4096]{2,1,0:T(8,128)(2,1)} async-done(((bf16[32,16,4096]{2,1,0:T(8,128)(2,1)}), bf16[4,16,4096]{2,1,0:T(8,128)(2,1)}) %reduce-scatter.5.cloned.1.call-update) | async-done | bytes 524304 | tf_op jit(solution)/shard_map/reduce_scatter | solution.py:142
  215.7 3.6 %all-to-all-start.1 = ((bf16[4,16,4096]{2,1,0:T(8,128)(2,1)}), bf16[4,16,4096]{2,1,0:T(8,128)(2,1)S(1)}, u32[]{:S(2)}, u32[]{:S(2)}) async-start(bf16[4,16,4096]{2,1,0:T(8,128)(2,1)} %reduce-scatter.5.cloned.1.call-done), calls=%async_computation.3 | async-start | bytes 1048576 | tf_op jit(solution)/shard_map/all_to_all | solution.py:148
  219.3 0.1 copy.92
  219.4 0.1 mul.208
  219.5 0.1 copy.88
  219.6 0.1 copy.85
  219.7 6.2 %all-to-all-done.1 = bf16[4,16,4096]{2,1,0:T(8,128)(2,1)S(1)} async-done(((bf16[4,16,4096]{2,1,0:T(8,128)(2,1)}), bf16[4,16,4096]{2,1,0:T(8,128)(2,1)S(1)}, u32[]{:S(2)}, u32[]{:S(2)}) %all-to-all-start.1) | async-done | bytes 524320 | tf_op jit(solution)/shard_map/all_to_all | solution.py:148
  225.9 0.7 gather_fusion
  226.6 0.2 gather.7
  226.8 0.8 multiply_reduce_fusion
  227.7 0.7 fusion.70
  (43 shorter events, 0.2 us)
Async XLA Ops:
  6.5 47.6 %copy-start = (bf16[256,4096]{1,0:T(8,128)(2,1)S(1)}, bf16[256,4096]{1,0:T(8,128)(2,1)}, u32[]{:S(2)}) copy-start(bf16[256,4096]{1,0:T(8,128)(2,1)} %param.28) | copy-start | bytes 6291460
  6.5 26.5 %copy-start.13 = (f32[2,2]{1,0:T(2,128)S(1)}, f32[2,2]{1,0:T(2,128)}, u32[]{:S(2)}) copy-start(f32[2,2]{1,0:T(2,128)} %param.24) | copy-start | bytes 52
  6.5 83.1 %reduce-scatter.3.cloned.1.call-start = ((), (), s32[]{:S(2)}) async-start(), calls=%async_computation.4 | async-start | bytes 1179648 | tf_op jit(solution)/shard_map/reduce_scatter | solution.py:101
  19.1 15.1 %copy-start.7 = (bf16[128,2,128]{2,1,0:T(2,128)(2,1)S(1)}, bf16[128,2,128]{2,1,0:T(2,128)(2,1)}, u32[]{:S(2)}) copy-start(bf16[128,2,128]{2,1,0:T(2,128)(2,1)} %param.22) | copy-start | bytes 196612
  20.1 22.8 %copy-start.6 = (bf16[128,2,128]{2,1,0:T(2,128)(2,1)S(1)}, bf16[128,2,128]{2,1,0:T(2,128)(2,1)}, u32[]{:S(2)}) copy-start(bf16[128,2,128]{2,1,0:T(2,128)(2,1)} %param.21) | copy-start | bytes 196612
  20.8 22.8 %copy-start.8 = (bf16[128,2,128]{2,1,0:T(2,128)(2,1)S(1)}, bf16[128,2,128]{2,1,0:T(2,128)(2,1)}, u32[]{:S(2)}) copy-start(bf16[128,2,128]{2,1,0:T(2,128)(2,1)} %param.23) | copy-start | bytes 196612
  33.0 21.1 %copy-start.14 = (f32[128]{0:T(128)S(1)}, f32[128]{0:T(128)}, u32[]{:S(2)}) copy-start(f32[128]{0:T(128)} %param.26) | copy-start | bytes 1540
  33.2 0.8 copy-start.2
  43.8 10.9 %copy-start.1 = (bf16[512,4096]{1,0:T(8,128)(2,1)S(1)}, bf16[512,4096]{1,0:T(8,128)(2,1)}, u32[]{:S(2)}) copy-start(bf16[512,4096]{1,0:T(8,128)(2,1)} %param.27) | copy-start | bytes 12582916
  43.8 10.9 %copy-start.3 = (f32[2,2,128,256]{3,2,1,0:T(8,128)S(1)}, f32[2,2,128,256]{3,2,1,0:T(8,128)}, u32[]{:S(2)}) copy-start(f32[2,2,128,256]{3,2,1,0:T(8,128)} %copy-done.2) | copy-start | bytes 1572868
  43.8 10.9 %copy-start.11 = (f32[256]{0:T(256)S(1)}, f32[256]{0:T(256)}, u32[]{:S(2)}) copy-start(f32[256]{0:T(256)} %param.25) | copy-start | bytes 3076
  54.7 1.9 copy-start.10
  54.7 34.9 %copy-start.4 = (bf16[16,4096]{1,0:T(8,128)(2,1)S(1)}, bf16[16,4096]{1,0:T(8,128)(2,1)}, u32[]{:S(2)}) copy-start(bf16[16,4096]{1,0:T(8,128)(2,1)} %param.29) | copy-start | bytes 393220
  54.7 35.9 %copy-start.9 = (f32[4096]{0:T(1024)S(1)}, f32[4096]{0:T(1024)}, u32[]{:S(2)}) copy-start(f32[4096]{0:T(1024)} %param.30) | copy-start | bytes 49156
  56.6 91.7 %all-gather.2.cloned.1.call-start = ((), (), s32[]{:S(2)}) async-start(), calls=%async_computation.5 | async-start | bytes 4718592 | tf_op jit(solution)/shard_map/all_gather | solution.py:136
  102.9 112.8 %reduce-scatter.5.cloned.1.call-start = ((), (), s32[]{:S(2)}) async-start(), calls=%async_computation.6 | async-start | bytes 4718592 | tf_op jit(solution)/shard_map/reduce_scatter | solution.py:142
  166.8 52.8 %copy-start.12 = (f32[16,2]{0,1:T(2,128)S(1)}, f32[16,2]{0,1:T(2,128)}, u32[]{:S(2)}) copy-start(f32[16,2]{0,1:T(2,128)} %param.32) | copy-start | bytes 388
  166.8 60.9 %copy-start.5 = (bf16[16,4096]{1,0:T(8,128)(2,1)S(1)}, bf16[16,4096]{1,0:T(8,128)(2,1)}, u32[]{:S(2)}) copy-start(bf16[16,4096]{1,0:T(8,128)(2,1)} %reduce-scatter.3.cloned.1.call-done) | copy-start | bytes 393220
  215.7 10.2 %all-to-all-start.1 = ((bf16[4,16,4096]{2,1,0:T(8,128)(2,1)}), bf16[4,16,4096]{2,1,0:T(8,128)(2,1)S(1)}, u32[]{:S(2)}, u32[]{:S(2)}) async-start(bf16[4,16,4096]{2,1,0:T(8,128)(2,1)} %reduce-scatter.5.cloned.1.call-done), calls=%async_computation.3 | async-start | bytes 1048576 | tf_op jit(solution)/shard_map/all_to_all | solution.py:148
Sparse Core Ops, SparseCore 0:
  56.7 32.8 reduce-scatter.2
  103.0 45.2 all-gather.1
  166.9 48.7 reduce-scatter.4
where the time goes:
time: 235 us
  waiting for transfers between devices  133 us (57%)
  blocking collectives  50.2 us (21%)
  matrix products  19.9 us (8%)
  between operations  13.5 us (6%)
  local copies, waits for them, and re-layouts  10.5 us (4%)
  other arithmetic  4.46 us (2%)
  starting transfers between devices  3.72 us (2%)
    reduce_scatter x1, waiting for transfers between devices, per_device(): lax.psum_scatter(partial_value.astype(jnp.float32).astype(jnp.bfloat16),...  48.9 us
    all_gather x1, waiting for transfers between devices, per_device(): pieces = lax.all_gather(arrived, 'tp', axis=0, tiled=True)  45.4 us
    reduce_scatter x1, waiting for transfers between devices, per_device(): lax.psum_scatter((first + jnp.einsum('hqv,hvd->qd', attended_b, weights_b...  32.2 us
    all_gather x1, blocking collectives, per_device(): keys_a = lax.all_gather(key_a, 'sp', axis=0, tiled=True)  11.5 us
    all_to_all x1, blocking collectives, per_device(): lax.all_to_all(outgoing, 'sp', split_axis=0, concat_axis=0, tiled=True)  11 us
    all_gather x1, blocking collectives, per_device(): values_a = lax.all_gather(value_a, 'sp', axis=0, tiled=True)  10.2 us
    dot_general x1, matrix products, per_device(): jnp.einsum('necf,efd->necd', active, w_down, preferred_element_type=jnp.f...  9.1 us
    all_gather x1, blocking collectives, per_device(): values_b = lax.all_gather(value_b, 'sp', axis=0, tiled=True)  9.03 us
  transfers between devices with their start and end apart: 4, of which 4 were waited for; matrix products, arithmetic and copies ran while one was open for 0% of the time, Pallas kernels for 0%

commit v1 on v0

--- a/solution.py
+++ b/solution.py
@@ -1,6 +1,10 @@
+import functools
+
 import jax
 import jax.numpy as jnp
 from jax import lax
+from jax.experimental import pallas as pl
+from jax.experimental.pallas import tpu as pltpu
 from jax.sharding import PartitionSpec as P
 
 EPSILON = 1e-06
@@ -58,7 +62,7 @@
     ).astype(jnp.bfloat16)
 
 
-def per_device(
+def per_device_plain(
     query_a,
     key_a,
     value_a,
@@ -156,6 +160,453 @@
     return (widened + combined).astype(jnp.bfloat16)
 
 
+def layer_kernel(
+    dims,
+    kv_ref,
+    q_ref,
+    lam_ref,
+    gain_a_ref,
+    gain_b_ref,
+    res_ref,
+    norm_ref,
+    route_ref,
+    out_a_hbm,
+    out_b_hbm,
+    gate_hbm,
+    up_hbm,
+    down_hbm,
+    o_ref,
+    kv_all,
+    out_a,
+    out_b,
+    w_gate,
+    w_up,
+    w_down,
+    att_a,
+    att_b,
+    part,
+    pair1,
+    sum1,
+    z1,
+    mixed,
+    x_all,
+    act,
+    contrib,
+    pair2,
+    red,
+    sp2,
+    z2s,
+    z2,
+    tot,
+    loc_sem,
+    kv_s,
+    kv_r,
+    p1_s,
+    p1_r,
+    z1_s,
+    z1_r,
+    gz_s,
+    gz_r,
+    gs_s,
+    gs_r,
+    gp_s,
+    gp_r,
+    p2_s,
+    p2_r,
+    s2_s,
+    s2_r,
+    z2_s,
+    z2_r,
+):
+    n_sp, n_tp, heads, da, db, va, vb = dims
+    nz = n_tp // 2
+    f32, bf16 = jnp.float32, jnp.bfloat16
+    sp = lax.axis_index("sp")
+    tp = lax.axis_index("tp")
+    z, core = tp // 2, tp % 2
+    rows, width = res_ref.shape
+    chunk = nz * 2 * rows
+    experts_here, _, hidden = w_gate.shape
+    experts_all = experts_here * n_sp
+
+    def sp_at(e):
+        return lax.rem(sp + e + n_sp, n_sp)
+
+    def z_at(d):
+        return lax.rem(z + d + nz, nz)
+
+    partner = {"sp": sp, "tp": z * 2 + 1 - core}
+
+    def to_sp(e):
+        return {"sp": sp_at(e), "tp": tp}
+
+    def to_z(d):
+        return {"sp": sp, "tp": z_at(d) * 2 + core}
+
+    def remote(src, dst, send, recv, device):
+        return pltpu.make_async_remote_copy(
+            src_ref=src,
+            dst_ref=dst,
+            send_sem=send,
+            recv_sem=recv,
+            device_id=device,
+            device_id_type=pl.DeviceIdType.MESH,
+        )
+
+    def kv_copy(e):
+        return remote(kv_ref, kv_all.at[sp], kv_s.at[e - 1], kv_r.at[e - 1], to_sp(e))
+
+    def p1_copy(d):
+        zz = z_at(d)
+        return remote(part.at[1 - core, zz], pair1.at[zz], p1_s.at[d], p1_r.at[d], partner)
+
+    def z1_copy(d):
+        return remote(sum1.at[z_at(d)], z1.at[d - 1], z1_s.at[d - 1], z1_r.at[d - 1], to_z(d))
+
+    def gz_copy(d):
+        block = x_all.at[sp, z, core]
+        return remote(block, block, gz_s.at[d - 1], gz_r.at[d - 1], to_z(d))
+
+    def gs_copy(e, d):
+        block = x_all.at[sp, z_at(-d), core]
+        return remote(block, block, gs_s.at[e - 1, d], gs_r.at[e - 1, d], to_sp(e))
+
+    def gp_copy(e, d):
+        block = x_all.at[sp_at(-e), z_at(-d), core]
+        return remote(block, block, gp_s.at[e, d], gp_r.at[e, d], partner)
+
+    def p2_copy(e):
+        return remote(contrib.at[e, 1 - core], pair2.at[e], p2_s.at[e], p2_r.at[e], partner)
+
+    def s2_copy(e, d):
+        zz = z_at(d)
+        return remote(
+            red.at[e, zz], sp2.at[e - 1, zz], s2_s.at[e - 1, d], s2_r.at[e - 1, d], to_sp(-e)
+        )
+
+    def z2_copy(d):
+        return remote(z2s.at[d - 1], z2.at[d - 1], z2_s.at[d - 1], z2_r.at[d - 1], to_z(d))
+
+    barrier = pltpu.get_barrier_semaphore()
+    for e in range(1, n_sp):
+        pl.semaphore_signal(
+            barrier, inc=1, device_id=to_sp(e), device_id_type=pl.DeviceIdType.MESH
+        )
+    for d in range(1, nz):
+        pl.semaphore_signal(barrier, inc=1, device_id=to_z(d), device_id_type=pl.DeviceIdType.MESH)
+    pl.semaphore_signal(barrier, inc=1, device_id=partner, device_id_type=pl.DeviceIdType.MESH)
+    pl.semaphore_wait(barrier, n_sp - 1 + nz - 1 + 1)
+
+    for e in range(1, n_sp):
+        kv_copy(e).start()
+    loads = [
+        pltpu.make_async_copy(src, dst, loc_sem.at[i])
+        for i, (src, dst) in enumerate(
+            (
+                (kv_ref, kv_all.at[sp]),
+                (out_a_hbm, out_a),
+                (out_b_hbm, out_b),
+                (gate_hbm, w_gate),
+                (up_hbm, w_up),
+                (down_hbm, w_down),
+            )
+        )
+    ]
+    for load in loads:
+        load.start()
+    loads[0].wait()
+    for e in range(1, n_sp):
+        kv_copy(e).wait_recv()
+
+    positions = kv_all.shape[1] * n_sp
+
+    def attend(q0, k0, v0, map_width, value_width, lam, gain):
+        heard = []
+        for which in range(2):
+            if map_width % 128 == 0:
+                query = q_ref[:, q0 + which * map_width : q0 + (which + 1) * map_width]
+                keys = kv_all[:, :, k0 + which * map_width : k0 + (which + 1) * map_width]
+            else:
+                query = q_ref[:, q0 : q0 + 2 * map_width]
+                lane = lax.broadcasted_iota(jnp.int32, query.shape, 1)
+                inside = (lane >= which * map_width) & (lane < (which + 1) * map_width)
+                query = jnp.where(inside, query.astype(f32), 0.0).astype(bf16)
+                keys = kv_all[:, :, k0 : k0 + 2 * map_width]
+            keys = keys.reshape(positions, keys.shape[2])
+            scores = lax.dot_general(
+                query, keys, (((1,), (1,)), ((), ())), preferred_element_type=f32
+            ) * (map_width**-0.5)
+            expo = jnp.exp(scores - jnp.max(scores, axis=1, keepdims=True))
+            total = jnp.sum(expo, axis=1, keepdims=True)
+            values = kv_all[:, :, v0 : v0 + value_width].reshape(positions, value_width)
+            carried = jnp.dot(expo.astype(bf16), values, preferred_element_type=f32)
+            heard.append(carried / total)
+        differ = heard[0] - lam * heard[1]
+        scaled = lax.rsqrt(jnp.mean(differ * differ, axis=1, keepdims=True) + EPSILON)
+        return (differ * scaled * gain).astype(bf16)
+
+    base_va = heads * 2 * da
+    base_kb = base_va + heads * va
+    base_vb = base_kb + heads * 2 * db
+    for h in range(heads):
+        att_a[:, h * va : (h + 1) * va] = attend(
+            h * 2 * da, h * 2 * da, base_va + h * va, da, va, lam_ref[0, h], gain_a_ref[...]
+        )
+    for h in range(heads):
+        att_b[:, h * vb : (h + 1) * vb] = attend(
+            heads * 2 * da + h * 2 * db,
+            base_kb + h * 2 * db,
+            base_vb + h * vb,
+            db,
+            vb,
+            lam_ref[1, h],
+            gain_b_ref[...],
+        )
+
+    loads[1].wait()
+    loads[2].wait()
+    tile = 512
+
+    @pl.loop(0, width // tile)
+    def _(j):
+        cols = pl.ds(pl.multiple_of(j * tile, tile), tile)
+        value = jnp.dot(att_a[...], out_a[:, cols], preferred_element_type=f32) + jnp.dot(
+            att_b[...], out_b[:, cols], preferred_element_type=f32
+        )
+        value = value.astype(bf16)
+        for zz in range(nz):
+            for c in range(2):
+                r = (zz * 2 + c) * rows
+                part[c, zz, :, cols] = value[r : r + rows]
+
+    order = list(range(1, nz)) + [0]
+    for d in order:
+        p1_copy(d).start()
+    for d in order:
+        p1_copy(d).wait_recv()
+        zz = z_at(d)
+        both = part[core, zz].astype(f32) + pair1[zz].astype(f32)
+        if d > 0:
+            sum1[zz] = both.astype(bf16)
+            z1_copy(d).start()
+        else:
+            tot[...] = both
+    for d in range(1, nz):
+        z1_copy(d).wait_recv()
+        tot[...] += z1[d - 1].astype(f32)
+    mix = (res_ref[...].astype(f32) + tot[...]).astype(bf16)
+    mixed[...] = mix
+    wide = mix.astype(f32)
+    scaled = lax.rsqrt(jnp.mean(wide * wide, axis=1, keepdims=True) + EPSILON)
+    x_all[sp, z, core, :, :width] = (wide * scaled * norm_ref[...]).astype(bf16)
+    route = route_ref[...]
+    high = route.astype(bf16)
+    lane = lax.broadcasted_iota(jnp.int32, route.shape, 1)
+    x_all[sp, z, core, :, width:] = jnp.where(
+        lane < experts_all, high.astype(f32), route - high.astype(f32)
+    ).astype(bf16)
+
+    for d in range(1, nz):
+        gz_copy(d).start()
+    for e in range(1, n_sp):
+        gs_copy(e, 0).start()
+    gp_copy(0, 0).start()
+    for d in range(1, nz):
+        gz_copy(d).wait_recv()
+        for e in range(1, n_sp):
+            gs_copy(e, d).start()
+        gp_copy(0, d).start()
+    for load in loads[3:]:
+        load.wait()
+
+    @pl.loop(0, n_sp)
+    def _(e):
+        @pl.when(e > 0)
+        def _():
+            for d in range(nz):
+                gs_copy(e, d).wait_recv()
+                gp_copy(e, d).start()
+
+        for d in range(nz):
+            gp_copy(e, d).wait_recv()
+        s = sp_at(-e)
+        share = x_all[s, :, :, :, width:].reshape(chunk, route.shape[1]).astype(f32)
+        lanes = lax.broadcasted_iota(jnp.int32, share.shape, 1)
+        for j in range(experts_here):
+            which = sp * experts_here + j
+            weight = jnp.sum(
+                jnp.where((lanes == which) | (lanes == which + experts_all), share, 0.0),
+                axis=1,
+                keepdims=True,
+            )
+            x = x_all[s, :, :, :, :width].reshape(chunk, width)
+            gate = jnp.dot(x, w_gate[j], preferred_element_type=f32)
+            upward = jnp.dot(x, w_up[j], preferred_element_type=f32)
+            clamped = jnp.minimum(gate, LIMIT)
+            active = (
+                clamped * jax.nn.sigmoid(SLOPE * clamped) * (jnp.clip(upward, -LIMIT, LIMIT) + 1.0)
+            )
+            act[:, j * hidden : (j + 1) * hidden] = (active * weight).astype(bf16)
+
+        @pl.loop(0, width // tile)
+        def _(i):
+            cols = pl.ds(pl.multiple_of(i * tile, tile), tile)
+            rowsum = jnp.zeros((chunk, tile), f32)
+            for j in range(experts_here):
+                rowsum += jnp.dot(
+                    act[:, j * hidden : (j + 1) * hidden],
+                    w_down[j, :, cols],
+                    preferred_element_type=f32,
+                )
+            value = rowsum.astype(bf16)
+            for zz in range(nz):
+                for c in range(2):
+                    r = (zz * 2 + c) * rows
+                    contrib[e, c, zz, :, cols] = value[r : r + rows]
+
+        p2_copy(e).start()
+        p2_copy(e).wait_recv()
+        for d in order:
+            zz = z_at(d)
+            red[e, zz] = (contrib[e, core, zz].astype(f32) + pair2[e, zz].astype(f32)).astype(bf16)
+
+            @pl.when(e > 0)
+            def _():
+                s2_copy(e, d).start()
+
+    for d in order:
+        zz = z_at(d)
+        total = red[0, zz].astype(f32)
+        for e in range(1, n_sp):
+            s2_copy(e, d).wait_recv()
+            total += sp2[e - 1, zz].astype(f32)
+        if d > 0:
+            z2s[d - 1] = total.astype(bf16)
+            z2_copy(d).start()
+        else:
+            tot[...] = total
+    for d in range(1, nz):
+        z2_copy(d).wait_recv()
+        tot[...] += z2[d - 1].astype(f32)
+    o_ref[...] = (mixed[...].astype(f32) + tot[...]).astype(bf16)
+
+    for e in range(1, n_sp):
+        kv_copy(e).wait_send()
+    for d in range(nz):
+        p1_copy(d).wait_send()
+    for d in range(1, nz):
+        z1_copy(d).wait_send()
+        gz_copy(d).wait_send()
+        z2_copy(d).wait_send()
+    for e in range(n_sp):
+        p2_copy(e).wait_send()
+        for d in range(nz):
+            gp_copy(e, d).wait_send()
+            if e > 0:
+                gs_copy(e, d).wait_send()
+                s2_copy(e, d).wait_send()
+
+
+def per_device(
+    n_sp,
+    n_tp,
+    query_a,
+    key_a,
+    value_a,
+    query_b,
+    key_b,
+    value_b,
+    lambdas,
+    gain_a,
+    gain_b,
+    out_a,
+    out_b,
+    residual,
+    norm_gain,
+    route_ids,
+    route_weights,
+    w_gate,
+    w_up,
+    w_down,
+):
+    here, heads, _ = query_a.shape
+    da, db = query_a.shape[2] // 2, query_b.shape[2] // 2
+    va, vb = value_a.shape[2], value_b.shape[2]
+    rows, width = residual.shape
+    experts_here, _, hidden = w_gate.shape
+    experts_all = experts_here * n_sp
+    nz = n_tp // 2
+    bf16, f32 = jnp.bfloat16, jnp.float32
+
+    def flat(*arrays):
+        return jnp.concatenate([a.reshape(here, -1) for a in arrays], axis=1)
+
+    kv = flat(key_a, value_a, key_b, value_b)
+    queries = flat(query_a, query_b)
+    chosen = route_ids[:, :, None] == jnp.arange(experts_all, dtype=jnp.int32)
+    dense = jnp.sum(jnp.where(chosen, route_weights[:, :, None], 0.0), axis=1)
+    lanes = -(-2 * experts_all // 128) * 128
+    route = jnp.concatenate(
+        [dense, dense, jnp.zeros((rows, lanes - 2 * experts_all), f32)], axis=1
+    )
+    vmem = pl.BlockSpec(memory_space=pltpu.VMEM)
+    hbm = pl.BlockSpec(memory_space=pl.ANY)
+    sem = pltpu.SemaphoreType.DMA
+    pairs = [(n_sp - 1,), (nz,), (nz - 1,), (nz - 1,), (n_sp - 1, nz), (n_sp, nz), (n_sp,)]
+    pairs += [(n_sp - 1, nz), (nz - 1,)]
+    scratch = [
+        pltpu.VMEM((n_sp,) + kv.shape, bf16),
+        pltpu.VMEM(out_a.shape, bf16),
+        pltpu.VMEM(out_b.shape, bf16),
+        pltpu.VMEM(w_gate.shape, bf16),
+        pltpu.VMEM(w_up.shape, bf16),
+        pltpu.VMEM(w_down.shape, bf16),
+        pltpu.VMEM((here, heads * va), bf16),
+        pltpu.VMEM((here, heads * vb), bf16),
+        pltpu.VMEM((2, nz, rows, width), bf16),
+        pltpu.VMEM((nz, rows, width), bf16),
+        pltpu.VMEM((nz, rows, width), bf16),
+        pltpu.VMEM((nz - 1, rows, width), bf16),
+        pltpu.VMEM((rows, width), bf16),
+        pltpu.VMEM((n_sp, nz, 2, rows, width + lanes), bf16),
+        pltpu.VMEM((n_tp * rows, experts_here * hidden), bf16),
+        pltpu.VMEM((n_sp, 2, nz, rows, width), bf16),
+        pltpu.VMEM((n_sp, nz, rows, width), bf16),
+        pltpu.VMEM((n_sp, nz, rows, width), bf16),
+        pltpu.VMEM((n_sp - 1, nz, rows, width), bf16),
+        pltpu.VMEM((nz - 1, rows, width), bf16),
+        pltpu.VMEM((nz - 1, rows, width), bf16),
+        pltpu.VMEM((rows, width), f32),
+        sem((6,)),
+    ]
+    for shape in pairs:
+        scratch += [sem(shape), sem(shape)]
+    return pl.pallas_call(
+        functools.partial(layer_kernel, (n_sp, n_tp, heads, da, db, va, vb)),
+        out_shape=jax.ShapeDtypeStruct((rows, width), bf16),
+        in_specs=[vmem, vmem, pl.BlockSpec(memory_space=pltpu.SMEM)] + [vmem] * 5 + [hbm] * 5,
+        out_specs=vmem,
+        scratch_shapes=scratch,
+        compiler_params=pltpu.CompilerParams(
+            collective_id=0, has_side_effects=True, vmem_limit_bytes=60 * 1024 * 1024
+        ),
+    )(
+        kv,
+        queries,
+        lambdas,
+        gain_a.reshape(1, -1),
+        gain_b.reshape(1, -1),
+        residual,
+        norm_gain.reshape(1, -1),
+        route,
+        out_a,
+        out_b,
+        w_gate,
+        w_up,
+        w_down,
+    )
+
+
 def solution(mesh):
     in_specs = (
         P("sp", "tp", None),
@@ -178,6 +629,9 @@
         P("sp", "tp", None),
     )
     out_specs = P(("sp", "tp"), None)
+    n_sp, n_tp = mesh.shape["sp"], mesh.shape["tp"]
+    fits = n_tp % 2 == 0 and n_sp * n_tp <= 32
+    body = functools.partial(per_device, n_sp, n_tp) if fits else per_device_plain
     return jax.shard_map(
-        per_device, mesh=mesh, in_specs=in_specs, out_specs=out_specs, check_vma=False
-    )
+        body, mesh=mesh, in_specs=in_specs, out_specs=out_specs, check_vma=False
+    )

time: 235 us -> 119 us (0.51)
  waiting for transfers between devices: 133 us -> 0 us
  Pallas kernels: 0 us -> 108 us
  blocking collectives: 50.2 us -> 0 us
  matrix products: 19.9 us -> 0 us
  between operations: 13.5 us -> 0.03 us
  local copies, waits for them, and re-layouts: 10.5 us -> 6.22 us
  starting transfers between devices: 3.72 us -> 0 us
    pallas_call x0 -> x1, Pallas kernels: none -> 108 us  [per_device(): pl.pallas_call(functools.partial(layer_kernel, (n_sp, n_tp, heads, da, db...]
    reduce_scatter x2 -> x0, waiting for transfers between devices: 81.1 us -> none  [the longest x1 48.9 us: per_device(): lax.psum_scatter(partial_value.astype(jnp.float32).astype(jnp.bfloat16),...]
    all_gather x1 -> x0, waiting for transfers between devices: 45.4 us -> none  [per_device(): pieces = lax.all_gather(arrived, 'tp', axis=0, tiled=True)]
    all_gather x4 -> x0, blocking collectives: 39.3 us -> none  [the longest x1 11.5 us: per_device(): keys_a = lax.all_gather(key_a, 'sp', axis=0, tiled=True)]
    dot_general x13 -> x0, matrix products: 19.9 us -> none  [the longest x1 9.1 us: per_device(): jnp.einsum('necf,efd->necd', active, w_down, preferred_element_type=jnp.f...]
    all_to_all x1 -> x0, blocking collectives: 11 us -> none  [per_device(): lax.all_to_all(outgoing, 'sp', split_axis=0, concat_axis=0, tiled=True)]
    all_to_all x1 -> x0, waiting for transfers between devices: 6.2 us -> none  [per_device(): lax.all_to_all(totals, 'sp', split_axis=0, concat_axis=0, tiled=True)]
    convert_element_type x1 -> x0, local copies, waits for them, and re-layouts: 4.61 us -> none  [per_device(): down.astype(jnp.bfloat16).reshape(count, slots_here, model_width)]
  transfers between devices with their start and end apart: 4 -> 0, of which waited for: 4 -> 0; matrix products, arithmetic and copies ran while one was open for 0% -> 0% of each run, Pallas kernels for 0% -> 0%
where the time goes in v1:
time: 119 us; the launch traced here: 117 us
  Pallas kernels  108 us (91%)
  local copies, waits for them, and re-layouts  6.22 us (5%)
  other arithmetic  2.83 us (2%)
    pallas_call x1, Pallas kernels, per_device(): pl.pallas_call(functools.partial(layer_kernel, (n_sp, n_tp, heads, da, db...  108 us
    unnamed x5, local copies, waits for them, and re-layouts  5.18 us

profile of v1, /device:TPU:0, one launch (start us, length us, event | category | flops | bytes accessed | tf_op | source)
XLA Modules:
  0.0 117.2 jit_solution(13888447563249930931)
XLA Ops:
  0.0 0.9 copy_bitcast_fusion.1
  0.9 0.9 copy.23
  1.8 0.9 copy.24
  2.7 0.8 pad_maximum_fusion.kv_ref
  3.5 0.9 copy.27
  4.4 0.9 copy.32
  5.3 0.7 pad_maximum_fusion.1.q_ref
  6.0 0.7 select_reduce_fusion
  6.7 0.1 copy.21
  6.7 0.1 pad.2.clone
  6.8 0.7 maximum_maximum_fusion.route_ref
  7.5 108.2 %shard_map.172 = bf16[16,4096]{1,0:T(8,128)(2,1)} custom-call(bf16[128,1536]{1,0:T(8,128)(2,1)} %pad_maximum_fusion.kv_ref, bf16[128,768]{1,0:T(8,128)(2,1)} %pad_maximum_fusion.1.q_ref, f32[2,2]{1,0:T(2,128)} %lam_ref.1, f32[1,256]{1,0:T(1,128)} %bitcast.30, f32[1,128]{1,0:T(1,128)} %bitcast.31, bf16[16,4096]{1,0:T(8,128)(2,1)} %res_ref.1, ...), custom_call_target="tpu_custom_call" | custom-call | tf_op jit(solution)/shard_map/pallas_call | solution.py:584
  115.7 1.6 %copy.34 = bf16[16,4096]{1,0:T(8,128)(2,1)} copy(bf16[16,4096]{1,0:T(8,128)(2,1)} %shard_map.172) | data formatting | bytes 262144
  (1 shorter events, 0.0 us)

commit v2 on v1

--- a/solution.py
+++ b/solution.py
@@ -225,7 +225,7 @@
     tp = lax.axis_index("tp")
     z, core = tp // 2, tp % 2
     rows, width = res_ref.shape
-    chunk = nz * 2 * rows
+    chunk = n_sp * 2 * rows
     experts_here, _, hidden = w_gate.shape
     experts_all = experts_here * n_sp
 
@@ -253,8 +253,23 @@
             device_id_type=pl.DeviceIdType.MESH,
         )
 
-    def kv_copy(e):
-        return remote(kv_ref, kv_all.at[sp], kv_s.at[e - 1], kv_r.at[e - 1], to_sp(e))
+    x_next = sp + 1 - 2 * (sp % 2)
+    y_next = lax.rem(sp + 2, n_sp)
+
+    def kv_copy(i):
+        owner, target, half = (
+            (sp, x_next, 0),
+            (sp, y_next, 1),
+            (sp, x_next, 1),
+            (sp, y_next, 0),
+            (x_next, y_next, 0),
+            (y_next, x_next, 1),
+        )[i]
+        size = kv_ref.shape[0] // 2
+        part_rows = pl.ds(half * size, size)
+        place = kv_all.at[owner, part_rows]
+        source = kv_ref.at[part_rows] if i < 4 else place
+        return remote(source, place, kv_s.at[i], kv_r.at[i], {"sp": target, "tp": tp})
 
     def p1_copy(d):
         zz = z_at(d)
@@ -264,28 +279,27 @@
         return remote(sum1.at[z_at(d)], z1.at[d - 1], z1_s.at[d - 1], z1_r.at[d - 1], to_z(d))
 
     def gz_copy(d):
-        block = x_all.at[sp, z, core]
+        block = x_all.at[z, sp, core]
         return remote(block, block, gz_s.at[d - 1], gz_r.at[d - 1], to_z(d))
 
     def gs_copy(e, d):
-        block = x_all.at[sp, z_at(-d), core]
+        block = x_all.at[z_at(-d), sp, core]
         return remote(block, block, gs_s.at[e - 1, d], gs_r.at[e - 1, d], to_sp(e))
 
     def gp_copy(e, d):
-        block = x_all.at[sp_at(-e), z_at(-d), core]
+        block = x_all.at[z_at(-d), sp_at(-e), core]
         return remote(block, block, gp_s.at[e, d], gp_r.at[e, d], partner)
 
-    def p2_copy(e):
-        return remote(contrib.at[e, 1 - core], pair2.at[e], p2_s.at[e], p2_r.at[e], partner)
+    def p2_copy(d):
+        return remote(contrib.at[d, 1 - core], pair2.at[d], p2_s.at[d], p2_r.at[d], partner)
 
     def s2_copy(e, d):
-        zz = z_at(d)
         return remote(
-            red.at[e, zz], sp2.at[e - 1, zz], s2_s.at[e - 1, d], s2_r.at[e - 1, d], to_sp(-e)
+            red.at[d, sp_at(e)], sp2.at[e - 1, d], s2_s.at[e - 1, d], s2_r.at[e - 1, d], to_sp(e)
         )
 
     def z2_copy(d):
-        return remote(z2s.at[d - 1], z2.at[d - 1], z2_s.at[d - 1], z2_r.at[d - 1], to_z(d))
+        return remote(z2s.at[d - 1], z2.at[d - 1], z2_s.at[d - 1], z2_r.at[d - 1], to_z(-d))
 
     barrier = pltpu.get_barrier_semaphore()
     for e in range(1, n_sp):
@@ -297,8 +311,8 @@
     pl.semaphore_signal(barrier, inc=1, device_id=partner, device_id_type=pl.DeviceIdType.MESH)
     pl.semaphore_wait(barrier, n_sp - 1 + nz - 1 + 1)
 
-    for e in range(1, n_sp):
-        kv_copy(e).start()
+    for i in range(4):
+        kv_copy(i).start()
     loads = [
         pltpu.make_async_copy(src, dst, loc_sem.at[i])
         for i, (src, dst) in enumerate(
@@ -315,8 +329,11 @@
     for load in loads:
         load.start()
     loads[0].wait()
-    for e in range(1, n_sp):
-        kv_copy(e).wait_recv()
+    for i in range(2):
+        kv_copy(i).wait_recv()
+        kv_copy(4 + i).start()
+    for i in range(2, 6):
+        kv_copy(i).wait_recv()
 
     positions = kv_all.shape[1] * n_sp
 
@@ -398,11 +415,11 @@
     mixed[...] = mix
     wide = mix.astype(f32)
     scaled = lax.rsqrt(jnp.mean(wide * wide, axis=1, keepdims=True) + EPSILON)
-    x_all[sp, z, core, :, :width] = (wide * scaled * norm_ref[...]).astype(bf16)
+    x_all[z, sp, core, :, :width] = (wide * scaled * norm_ref[...]).astype(bf16)
     route = route_ref[...]
     high = route.astype(bf16)
     lane = lax.broadcasted_iota(jnp.int32, route.shape, 1)
-    x_all[sp, z, core, :, width:] = jnp.where(
+    x_all[z, sp, core, :, width:] = jnp.where(
         lane < experts_all, high.astype(f32), route - high.astype(f32)
     ).astype(bf16)
 
@@ -411,26 +428,40 @@
     for e in range(1, n_sp):
         gs_copy(e, 0).start()
     gp_copy(0, 0).start()
-    for d in range(1, nz):
-        gz_copy(d).wait_recv()
-        for e in range(1, n_sp):
-            gs_copy(e, d).start()
-        gp_copy(0, d).start()
     for load in loads[3:]:
         load.wait()
 
-    @pl.loop(0, n_sp)
-    def _(e):
-        @pl.when(e > 0)
+    def settle(d):
+        total = red[d, sp].astype(f32)
+        for e in range(1, n_sp):
+            s2_copy(e, d).wait_recv()
+            total += sp2[e - 1, d].astype(f32)
+
+        @pl.when(d > 0)
         def _():
-            for d in range(nz):
-                gs_copy(e, d).wait_recv()
-                gp_copy(e, d).start()
-
-        for d in range(nz):
+            z2s[d - 1] = total.astype(bf16)
+            z2_copy(d).start()
+
+        @pl.when(d == 0)
+        def _():
+            tot[...] = total
+
+    @pl.loop(0, nz)
+    def _(d):
+        @pl.when(d + 1 < nz)
+        def _():
+            gz_copy(d + 1).wait_recv()
+            for e in range(1, n_sp):
+                gs_copy(e, d + 1).start()
+            gp_copy(0, d + 1).start()
+
+        for e in range(1, n_sp):
+            gs_copy(e, d).wait_recv()
+            gp_copy(e, d).start()
+        for e in range(n_sp):
             gp_copy(e, d).wait_recv()
-        s = sp_at(-e)
-        share = x_all[s, :, :, :, width:].reshape(chunk, route.shape[1]).astype(f32)
+        zz = z_at(-d)
+        share = x_all[zz, :, :, :, width:].reshape(chunk, route.shape[1]).astype(f32)
         lanes = lax.broadcasted_iota(jnp.int32, share.shape, 1)
         for j in range(experts_here):
             which = sp * experts_here + j
@@ -439,7 +470,7 @@
                 axis=1,
                 keepdims=True,
             )
-            x = x_all[s, :, :, :, :width].reshape(chunk, width)
+            x = x_all[zz, :, :, :, :width].reshape(chunk, width)
             gate = jnp.dot(x, w_gate[j], preferred_element_type=f32)
             upward = jnp.dot(x, w_up[j], preferred_element_type=f32)
             clamped = jnp.minimum(gate, LIMIT)
@@ -459,48 +490,40 @@
                     preferred_element_type=f32,
                 )
             value = rowsum.astype(bf16)
-            for zz in range(nz):
+            for s in range(n_sp):
                 for c in range(2):
-                    r = (zz * 2 + c) * rows
-                    contrib[e, c, zz, :, cols] = value[r : r + rows]
-
-        p2_copy(e).start()
-        p2_copy(e).wait_recv()
-        for d in order:
-            zz = z_at(d)
-            red[e, zz] = (contrib[e, core, zz].astype(f32) + pair2[e, zz].astype(f32)).astype(bf16)
-
-            @pl.when(e > 0)
-            def _():
+                    r = (s * 2 + c) * rows
+                    contrib[d, c, s, :, cols] = value[r : r + rows]
+
+        p2_copy(d).start()
+        p2_copy(d).wait_recv()
+        for e in list(range(1, n_sp)) + [0]:
+            s = sp_at(e)
+            red[d, s] = (contrib[d, core, s].astype(f32) + pair2[d, s].astype(f32)).astype(bf16)
+            if e > 0:
                 s2_copy(e, d).start()
 
-    for d in order:
-        zz = z_at(d)
-        total = red[0, zz].astype(f32)
-        for e in range(1, n_sp):
-            s2_copy(e, d).wait_recv()
-            total += sp2[e - 1, zz].astype(f32)
-        if d > 0:
-            z2s[d - 1] = total.astype(bf16)
-            z2_copy(d).start()
-        else:
-            tot[...] = total
+        @pl.when(d > 0)
+        def _():
+            settle(d - 1)
+
+    settle(nz - 1)
     for d in range(1, nz):
         z2_copy(d).wait_recv()
         tot[...] += z2[d - 1].astype(f32)
     o_ref[...] = (mixed[...].astype(f32) + tot[...]).astype(bf16)
 
-    for e in range(1, n_sp):
-        kv_copy(e).wait_send()
+    for i in range(6):
+        kv_copy(i).wait_send()
     for d in range(nz):
         p1_copy(d).wait_send()
     for d in range(1, nz):
         z1_copy(d).wait_send()
         gz_copy(d).wait_send()
         z2_copy(d).wait_send()
-    for e in range(n_sp):
-        p2_copy(e).wait_send()
-        for d in range(nz):
+    for d in range(nz):
+        p2_copy(d).wait_send()
+        for e in range(n_sp):
             gp_copy(e, d).wait_send()
             if e > 0:
                 gs_copy(e, d).wait_send()
@@ -552,7 +575,7 @@
     vmem = pl.BlockSpec(memory_space=pltpu.VMEM)
     hbm = pl.BlockSpec(memory_space=pl.ANY)
     sem = pltpu.SemaphoreType.DMA
-    pairs = [(n_sp - 1,), (nz,), (nz - 1,), (nz - 1,), (n_sp - 1, nz), (n_sp, nz), (n_sp,)]
+    pairs = [(6,), (nz,), (nz - 1,), (nz - 1,), (n_sp - 1, nz), (n_sp, nz), (nz,)]
     pairs += [(n_sp - 1, nz), (nz - 1,)]
     scratch = [
         pltpu.VMEM((n_sp,) + kv.shape, bf16),
@@ -568,11 +591,11 @@
         pltpu.VMEM((nz, rows, width), bf16),
         pltpu.VMEM((nz - 1, rows, width), bf16),
         pltpu.VMEM((rows, width), bf16),
-        pltpu.VMEM((n_sp, nz, 2, rows, width + lanes), bf16),
-        pltpu.VMEM((n_tp * rows, experts_here * hidden), bf16),
-        pltpu.VMEM((n_sp, 2, nz, rows, width), bf16),
-        pltpu.VMEM((n_sp, nz, rows, width), bf16),
-        pltpu.VMEM((n_sp, nz, rows, width), bf16),
+        pltpu.VMEM((nz, n_sp, 2, rows, width + lanes), bf16),
+        pltpu.VMEM((n_sp * 2 * rows, experts_here * hidden), bf16),
+        pltpu.VMEM((nz, 2, n_sp, rows, width), bf16),
+        pltpu.VMEM((nz, n_sp, rows, width), bf16),
+        pltpu.VMEM((nz, n_sp, rows, width), bf16),
         pltpu.VMEM((n_sp - 1, nz, rows, width), bf16),
         pltpu.VMEM((nz - 1, rows, width), bf16),
         pltpu.VMEM((nz - 1, rows, width), bf16),
@@ -630,7 +653,7 @@
     )
     out_specs = P(("sp", "tp"), None)
     n_sp, n_tp = mesh.shape["sp"], mesh.shape["tp"]
-    fits = n_tp % 2 == 0 and n_sp * n_tp <= 32
+    fits = n_sp == 4 and n_tp % 2 == 0 and n_tp <= 8
     body = functools.partial(per_device, n_sp, n_tp) if fits else per_device_plain
     return jax.shard_map(
         body, mesh=mesh, in_specs=in_specs, out_specs=out_specs, check_vma=False

time: 119 us -> 109 us (0.916); the launches traced: 117 us -> 109 us
  Pallas kernels: 108 us -> 99.5 us
    pallas_call x1, Pallas kernels: 108 us -> 99.5 us  [per_device(): pl.pallas_call(functools.partial(layer_kernel, (n_sp, n_tp, heads, da, db...]
where the time goes in v2:
time: 109 us
  Pallas kernels  99.5 us (91%)
  local copies, waits for them, and re-layouts  6.22 us (6%)
  other arithmetic  2.83 us (3%)
    pallas_call x1, Pallas kernels, per_device(): pl.pallas_call(functools.partial(layer_kernel, (n_sp, n_tp, heads, da, db...  99.5 us
    unnamed x5, local copies, waits for them, and re-layouts  5.18 us

profile of v2, /device:TPU:0, one launch (start us, length us, event | category | flops | bytes accessed | tf_op | source)
XLA Modules:
  0.0 108.5 jit_solution(17779126632419140675)
XLA Ops:
  0.0 0.9 copy_bitcast_fusion.1
  0.9 0.9 copy.23
  1.8 0.9 copy.24
  2.7 0.8 pad_maximum_fusion.kv_ref
  3.5 0.9 copy.27
  4.4 0.9 copy.32
  5.3 0.7 pad_maximum_fusion.1.q_ref
  6.0 0.7 select_reduce_fusion
  6.7 0.1 copy.21
  6.7 0.1 pad.2.clone
  6.8 0.7 maximum_maximum_fusion.route_ref
  7.5 99.5 %shard_map.172 = bf16[16,4096]{1,0:T(8,128)(2,1)} custom-call(bf16[128,1536]{1,0:T(8,128)(2,1)} %pad_maximum_fusion.kv_ref, bf16[128,768]{1,0:T(8,128)(2,1)} %pad_maximum_fusion.1.q_ref, f32[2,2]{1,0:T(2,128)} %lam_ref.1, f32[1,256]{1,0:T(1,128)} %bitcast.30, f32[1,128]{1,0:T(1,128)} %bitcast.31, bf16[16,4096]{1,0:T(8,128)(2,1)} %res_ref.1, ...), custom_call_target="tpu_custom_call" | custom-call | tf_op jit(solution)/shard_map/pallas_call | solution.py:607
  107.0 1.6 %copy.34 = bf16[16,4096]{1,0:T(8,128)(2,1)} copy(bf16[16,4096]{1,0:T(8,128)(2,1)} %shard_map.172) | data formatting | bytes 262144
  (1 shorter events, 0.0 us)
